TPU v7x, 512 devices: a whole 4x4x16 slice. The times are simulated.
512 devices in a mesh: sp: 32 (over z, core), tp: 16 (over y, x).
Axes of the slice: x: 4, y: 4, z: 16, core: 2. Of those that a mesh axis runs over, the one named last changes fastest.
Arguments:
- query_proj: bfloat16 [8192, 2048], P('sp', 'tp'), may hold values from -4 to 4
- key_proj: bfloat16 [8192, 1024], P('sp', 'tp'), may hold values from -4 to 4
- value_proj: bfloat16 [8192, 1024], P('sp', 'tp'), may hold values from -48 to 48
- query_gain: float32 [32, 64], P('tp'), may hold values from 1 to 6
- key_gain: float32 [16, 64], P('tp'), may hold values from 1 to 6
- residual: bfloat16 [8192, 2048], P('sp', 'tp'), may hold values from -48 to 48
- out_weight: bfloat16 [2048, 2048], P(None, 'tp'), may hold values from -0.125 to 0.125
- route_expert: int32 [8192, 8], P('sp'), may hold values from 0 to 255, all different within a row; in each aligned block of 256 rows (0 to 255, 256 to 511, ...) at most 12 rows name the same one
- route_weight: float32 [8192, 8], P('sp'), may hold values from 0.25 to 1.25
- expert_gate: bfloat16 [512, 2048, 256], P(('sp', 'tp')), may hold values from -0.125 to 0.125
- expert_up: bfloat16 [512, 2048, 256], P(('sp', 'tp')), may hold values from -0.125 to 0.125
- expert_down: bfloat16 [512, 256, 2048], P(('sp', 'tp')), may hold values from -0.25 to 0.25
Outputs:
- block_out: bfloat16 [8192, 2048], P('sp', 'tp')
Inputs may be any that keep to these rules, and one draw needn't show every extreme that they name: `route_expert`: A row names 8 different experts; among the rows of one index of sp no expert is named by more than 12 rows, a bound that some block reaches of them.
All inputs are finite; a program needn't handle non-finite values.
Results may differ from a plain program's by a relative error of at most 0.012.
The roundings to bfloat16 on the way count: a program that leaves them out, or rounds other values in their place, can miss the bound.
Values may be sent and summed in bfloat16 or wider, within the bound.
A program may use at most 64 MiB of HBM per device.

v0:
```python
import math
import jax
import jax.numpy as jnp
from jax import lax
from jax.sharding import Mesh
from jax.sharding import PartitionSpec as P

HEAD_DIM = 64
TOP_K = 8
GRID_W = 64
SP = ("sp_0", "sp_1")
SP_TP = ("sp_0", "sp_1", "tp")
EPSILON = 1e-06
ROPE_BASE = 10000.0
KEY_BLOCK = 1024


def laid_out(pieces, dim):
    shape = list(pieces.shape[1:])
    shape[dim] *= pieces.shape[0]
    return jnp.moveaxis(pieces, 0, dim).reshape(shape)


def from_everyone(x, axis):
    devices = lax.axis_size(axis)
    return lax.all_to_all(jnp.broadcast_to(x[None], (devices, *x.shape)), axis, 0, 0, tiled=True)


def gather_directly(x, axis, dim):
    return laid_out(from_everyone(x, axis), dim)


def cut_along(x, dim, devices):
    shape = x.shape
    pieces = x.reshape(*shape[:dim], devices, shape[dim] // devices, *shape[dim + 1 :])
    return jnp.moveaxis(pieces, dim, 0)


def turned_blocks(pieces, axes, sequence):
    shape = [lax.axis_size(a) for a in axes]
    pieces = pieces.reshape(*shape, *pieces.shape[1:])
    for k in sequence:
        pieces = lax.all_to_all(pieces, axes[k], split_axis=k, concat_axis=k, tiled=True)
    return pieces.reshape(-1, *pieces.shape[len(axes) :])


def core_and_chips(x, groups, sequence, split_dim, concat_dim):
    devices = lax.axis_size(groups[0]) * lax.axis_size(groups[1])
    pieces = cut_along(x, split_dim, devices)
    return laid_out(turned_blocks(pieces, groups, sequence), concat_dim)


def swapped(value, axis, stride):
    mask = 2**stride
    pairs = [(source, source ^ mask) for source in range(lax.axis_size(axis))]
    return lax.ppermute(value, axis, pairs)


def summed_on_arrival(x, axis, dim):
    devices = lax.axis_size(axis)
    pieces = lax.all_to_all(cut_along(x, dim, devices), axis, 0, 0, tiled=True)
    return jnp.sum(pieces.astype(jnp.float32), axis=0)


def rotation_tables(offset, count):
    pair_count = HEAD_DIM // 4
    position = offset + jnp.arange(count, dtype=jnp.int32)
    grid_row = (position // GRID_W).astype(jnp.float32)
    grid_col = (position % GRID_W).astype(jnp.float32)
    inverse = ROPE_BASE ** (-jnp.arange(pair_count, dtype=jnp.float32) / pair_count)
    angles = jnp.stack([grid_row[:, None] * inverse, grid_col[:, None] * inverse], axis=1)
    return (jnp.cos(angles), jnp.sin(angles))


def rotate(vectors, cosine_table, sine_table):
    pair_count = HEAD_DIM // 4
    shaped = vectors.reshape(vectors.shape[:-1] + (2, 2, pair_count))
    first_half = shaped[..., 0, :]
    second_half = shaped[..., 1, :]
    cosine_row = cosine_table[:, None]
    sine_row = sine_table[:, None]
    turned = jnp.stack(
        [
            first_half * cosine_row - second_half * sine_row,
            first_half * sine_row + second_half * cosine_row,
        ],
        axis=-2,
    )
    return turned.reshape(vectors.shape)


def head_norm(vectors, gain):
    scaled = vectors.astype(jnp.float32)
    scaled = scaled * lax.rsqrt(jnp.mean(scaled * scaled, axis=-1, keepdims=True) + EPSILON)
    return scaled * gain


def online_update(running, query_groups, key_block, value_block):
    running_max, running_sum, running_acc = running
    scores = jnp.einsum(
        "tkgd,nkd->kgtn", query_groups, key_block, preferred_element_type=jnp.float32
    ) * HEAD_DIM ** (-0.5)
    new_max = jnp.maximum(running_max, jnp.max(scores, axis=-1))
    rescale = jnp.exp(running_max - new_max)
    weights = jnp.exp(scores - new_max[..., None]).astype(jnp.bfloat16)
    new_sum = running_sum * rescale + jnp.sum(weights.astype(jnp.float32), axis=-1)
    update = jnp.einsum("kgtn,nkd->kgtd", weights, value_block, preferred_element_type=jnp.float32)
    return (new_max, new_sum, running_acc * rescale[..., None] + update)


def local(
    query_proj,
    key_proj,
    value_proj,
    query_gain,
    key_gain,
    residual,
    out_weight,
    route_expert,
    route_weight,
    expert_gate,
    expert_up,
    expert_down,
):
    token_count = query_proj.shape[0]
    local_heads = query_gain.shape[0]
    local_kv = key_gain.shape[0]
    group_size = local_heads // local_kv
    sp_size = lax.axis_size(SP)
    tp_size = lax.axis_size("tp")
    tp_place = lax.axis_index("tp")
    offset = lax.axis_index(SP) * token_count
    cosine_table, sine_table = rotation_tables(offset, token_count)
    query_rot = rotate(
        head_norm(query_proj.reshape(token_count, local_heads, HEAD_DIM), query_gain),
        cosine_table,
        sine_table,
    ).astype(jnp.bfloat16)
    key_rot = rotate(
        head_norm(key_proj.reshape(token_count, local_kv, HEAD_DIM), key_gain),
        cosine_table,
        sine_table,
    ).astype(jnp.bfloat16)
    packed = jnp.concatenate(
        [key_rot.reshape(token_count, local_kv * HEAD_DIM), value_proj], axis=1
    )
    query_groups = query_rot.reshape(token_count, local_kv, group_size, HEAD_DIM)
    initial = (
        jnp.full((local_kv, group_size, token_count), -1e30, jnp.float32),
        jnp.zeros((local_kv, group_size, token_count), jnp.float32),
        jnp.zeros((local_kv, group_size, token_count, HEAD_DIM), jnp.float32),
    )
    incoming = lax.all_gather(packed, SP, axis=0, tiled=True)
    incoming_len = incoming.shape[0]
    step_len = math.gcd(incoming_len, KEY_BLOCK)

    def one_step(step_index, running):
        block_rows = lax.dynamic_slice_in_dim(incoming, step_index * step_len, step_len, 0)
        key_block = block_rows[:, : local_kv * HEAD_DIM].reshape(step_len, local_kv, HEAD_DIM)
        value_block = block_rows[:, local_kv * HEAD_DIM :].reshape(step_len, local_kv, HEAD_DIM)
        return online_update(running, query_groups, key_block, value_block)

    final_max, final_sum, final_acc = lax.fori_loop(0, incoming_len // step_len, one_step, initial)
    attended = final_acc / final_sum[..., None]
    attended = jnp.transpose(attended, (2, 0, 1, 3)).reshape(token_count, local_heads * HEAD_DIM)
    attended = attended.astype(jnp.bfloat16)
    projected = jnp.dot(
        gather_directly(attended, "tp", 1), out_weight, preferred_element_type=jnp.float32
    )
    mixed_sum = residual.astype(jnp.float32) + projected
    mixed_rows = mixed_sum.astype(jnp.bfloat16)
    full_rows = gather_directly(mixed_rows, "tp", 1)
    width_total = full_rows.shape[1]
    per_sp = tp_size // 2
    column = tp_place // 2
    half = tp_place % 2
    experts_total = per_sp * sp_size
    capacity = 3 * token_count * TOP_K // (2 * experts_total)
    slot_count = sp_size * capacity
    flat_choice = route_expert.reshape(token_count * TOP_K)
    onehot = (flat_choice[:, None] == jnp.arange(experts_total, dtype=jnp.int32)[None, :]).astype(
        jnp.int32
    )
    earlier = jnp.cumsum(onehot, axis=0) - onehot
    slot_rank = jnp.sum(earlier * onehot, axis=1)
    mine = flat_choice % per_sp == column
    target = flat_choice // per_sp * capacity + slot_rank
    owner = jnp.arange(token_count * TOP_K, dtype=jnp.int32) // TOP_K
    slot_token = (
        jnp.full((slot_count + 1,), token_count, jnp.int32)
        .at[jnp.where(mine, target, slot_count)]
        .set(owner)[:slot_count]
    )
    padded = jnp.concatenate([full_rows, jnp.zeros((1, width_total), jnp.bfloat16)], axis=0)
    selected = padded[slot_token].reshape(sp_size, capacity, width_total)
    half_cap = capacity // 2
    own_part = lax.dynamic_slice_in_dim(selected, half * half_cap, half_cap, 1)
    received = core_and_chips(own_part, ("sp_0", "sp_1"), (1, 0), 0, 0)
    partner = swapped(received, "tp", 0)
    arrived = jnp.where(
        half == 0,
        jnp.concatenate([received, partner], axis=1),
        jnp.concatenate([partner, received], axis=1),
    )
    expert_rows = arrived.reshape(slot_count, width_total)
    squares = jnp.mean(jnp.square(expert_rows.astype(jnp.float32)), axis=-1, keepdims=True)
    norm_scale = lax.rsqrt(squares + EPSILON)
    gate_value = (
        jnp.dot(expert_rows, expert_gate[0], preferred_element_type=jnp.float32) * norm_scale
    )
    up_value = jnp.dot(expert_rows, expert_up[0], preferred_element_type=jnp.float32) * norm_scale
    hidden = (jax.nn.silu(gate_value) * up_value).astype(jnp.bfloat16)
    half_result = jnp.dot(hidden, expert_down[0], preferred_element_type=jnp.float32).astype(
        jnp.bfloat16
    )
    returned = core_and_chips(
        half_result.reshape(sp_size, capacity, width_total), ("sp_0", "sp_1"), (1, 0), 0, 0
    )
    slot_results = returned.reshape(slot_count, width_total)
    mine_grid = mine.reshape(token_count, TOP_K)
    target_grid = target.reshape(token_count, TOP_K)
    gathered_sum = jnp.zeros((token_count, width_total), jnp.float32)
    for choice_index in range(TOP_K):
        chosen = mine_grid[:, choice_index]
        index = jnp.where(chosen, target_grid[:, choice_index], 0)
        factor = jnp.where(chosen, route_weight[:, choice_index], 0.0)
        picked = slot_results[index].astype(jnp.float32)
        gathered_sum = gathered_sum + factor[:, None] * picked
    routed = summed_on_arrival(gathered_sum.astype(jnp.bfloat16), "tp", 1)
    return (mixed_sum + routed).astype(jnp.bfloat16)


def solution(mesh):
    split = Mesh(mesh.devices.reshape(16, 2, mesh.shape["tp"]), ("sp_0", "sp_1", "tp"))
    in_specs = (
        P(SP, "tp"),
        P(SP, "tp"),
        P(SP, "tp"),
        P("tp", None),
        P("tp", None),
        P(SP, "tp"),
        P(None, "tp"),
        P(SP, None),
        P(SP, None),
        P(SP_TP, None, None),
        P(SP_TP, None, None),
        P(SP_TP, None, None),
    )
    out_specs = P(SP, "tp")
    return jax.shard_map(local, mesh=split, in_specs=in_specs, out_specs=out_specs, check_vma=False)
```

profile of v0, /device:TPU:2, one launch (start us, length us, event | category | flops | bytes accessed | tf_op | source)
XLA Modules:
  0.0 400.2 jit_solution(6346549353143653187)
XLA Ops:
  13.3 74.1 %all-gather.2.cloned.1.call-done = bf16[8192,128]{0,1:T(8,128)(2,1)} async-done(((bf16[256,128]{0,1:T(8,128)(2,1)}), bf16[8192,128]{0,1:T(8,128)(2,1)}) %all-gather.2.cloned.1.call-update) | async-done | bytes 2097168 | tf_op jit(solution)/shard_map/all_gather | solution.py:153
  87.4 25.7 %while.18 = (s32[]{:T(128)}, f32[1,2,256]{2,1,0:T(2,128)S(1)}, f32[1,2,256]{2,1,0:T(2,128)S(1)}, f32[1,2,256,64]{2,3,1,0:T(8,128)S(1)}, bf16[8192,128]{0,1:T(8,1...) while((s32[]{:T(128)}, f32[1,2,256]{2,1,0:T(2,128)S(1)}, ...), condition=%wide.region_5.6_spmd.clone, body=%wide.region_2.5_spmd.clone.sunk | while | flops 139561984 | bytes 6914247 | solution.py:163
  114.3 7.3 %all-to-all-start = ((bf16[16,256,128]{1,2,0:T(8,128)(2,1)}), bf16[16,256,128]{1,2,0:T(8,128)(2,1)}, u32[]{:S(2)}, u32[]{:S(2)}) async-start(bf16[16,256,128]{1,2,0:T(8,128)(2,1)} %broadcast_in_dim.47), calls=%async_computation | async-start | bytes 2097152 | tf_op jit(solution)/shard_map/all_to_all | solution.py:26
  123.4 14.4 %all-to-all-done = bf16[16,256,128]{1,2,0:T(8,128)(2,1)} async-done(((bf16[16,256,128]{1,2,0:T(8,128)(2,1)}), bf16[16,256,128]{1,2,0:T(8,128)(2,1)}, u32[]{:S(2)}, u32[]{:S(2)}) %all-to-all-start) | async-done | bytes 1048608 | tf_op jit(solution)/shard_map/all_to_all | solution.py:26
  140.9 5.8 %all-to-all-start.1 = ((bf16[16,256,128]{2,1,0:T(8,128)(2,1)}), bf16[16,256,128]{2,1,0:T(8,128)(2,1)}, u32[]{:S(2)}, u32[]{:S(2)}) async-start(bf16[16,256,128]{2,1,0:T(8,128)(2,1)} %broadcast_in_dim.49), calls=%async_computation.1 | async-start | bytes 2097152 | tf_op jit(solution)/shard_map/all_to_all | solution.py:26
  147.8 8.0 %scatter_custom_fusion = s32[385]{0:T(512)S(1)} fusion(s32[2048]{0:T(1024)S(1)} %bitcast.222, s32[2048]{0:T(1024)S(1)} %add_select_fusion.2, s32[]{:T(128)} %constant.176.clone.1), kind=kCustom, calls=%fused_computation.181 | custom fusion | bytes 1544 | tf_op jit(solution)/shard_map/scatter | solution.py:192
  155.8 6.1 %all-to-all-done.1 = bf16[16,256,128]{2,1,0:T(8,128)(2,1)} async-done(((bf16[16,256,128]{2,1,0:T(8,128)(2,1)}), bf16[16,256,128]{2,1,0:T(8,128)(2,1)}, u32[]{:S(2)}, u32[]{:S(2)}) %all-to-all-start.1) | async-done | bytes 1048608 | tf_op jit(solution)/shard_map/all_to_all | solution.py:26
  163.4 3.1 gather_fusion
  166.5 2.4 reshape.662
  169.8 4.4 %all_to_all.35 = bf16[16,2,1,6,2048]{4,0,3,2,1:T(8,128)(2,1)S(1)} all-to-all(bf16[16,2,1,6,2048]{4,0,3,2,1:T(8,128)(2,1)S(1)} %copy.136), channel_id=1, replica_groups=mesh['sp_0'=16,'sp_1'=2,'tp'=16] {'sp_1'}, dimensions={1} | all-to-all | bytes 1572864 | tf_op jit(solution)/shard_map/all_to_all | solution.py:43
  175.0 48.2 %all_to_all.36 = bf16[16,2,1,6,2048]{4,1,3,2,0:T(2,128)(2,1)S(1)} all-to-all(bf16[16,2,1,6,2048]{4,1,3,2,0:T(2,128)(2,1)S(1)} %copy.137), channel_id=1, replica_groups=mesh['sp_0'=16,'sp_1'=2,'tp'=16] {'sp_0'}, dimensions={0} | all-to-all | bytes 1572864 | tf_op jit(solution)/shard_map/all_to_all | solution.py:43
  224.0 3.8 collective-permute-start
  227.9 11.6 %collective-permute-done = bf16[32,6,2048]{2,0,1:T(8,128)(2,1)S(1)} collective-permute-done((bf16[32,6,2048]{2,0,1:T(8,128)(2,1)S(1)}, bf16[32,6,2048]{2,0,1:T(8,128)(2,1)S(1)}, u32[]{:S(2)}, u32[]{:S(2)}) %collective-permute-start) | collective-permute-done | bytes 786464 | tf_op jit(solution)/shard_map/ppermute | solution.py:56
  241.6 2.3 copy.139
  245.2 2.4 convolution_multiply_fusion
  247.7 4.2 %convolution_convert_fusion = bf16[384,2048]{1,0:T(8,128)(2,1)} fusion(bf16[1,256,2048]{2,1,0:T(8,128)(2,1)S(1)} %copy-done, f32[384,256]{1,0:T(8,128)S(1)} %convolution_multiply_fusion, bf16[384,2048]{1,0:T(8,128)(2,1)S(1)} %copy-done.1, bf16[1,2048,256]{2,1,0:T(8,128)(2,1)} %param.23, f32[384]{0:T(512)S(1)} %rsqrt.30), kind=kOutput, calls=%fused_computation.32 | convolution fusion | flops 806780928 | bytes 5637632 | tf_op jit(solution)/shard_map/dot_general | solution.py:213
  251.8 2.4 reshape_reshape_reshape.6
  255.1 5.0 %all_to_all.37 = bf16[16,2,1,12,2048]{4,0,3,2,1:T(8,128)(2,1)S(1)} all-to-all(bf16[16,2,1,12,2048]{4,0,3,2,1:T(8,128)(2,1)S(1)} %copy.141), channel_id=1, replica_groups=mesh['sp_0'=16,'sp_1'=2,'tp'=16] {'sp_1'}, dimensions={1} | all-to-all | bytes 3145728 | tf_op jit(solution)/shard_map/all_to_all | solution.py:43
  260.1 2.8 copy.142
  262.9 11.4 %all-to-all-start.5 = ((bf16[16,2,1,12,2048]{4,1,3,2,0:T(2,128)(2,1)}), bf16[16,2,1,12,2048]{4,1,3,2,0:T(2,128)(2,1)S(1)}, u32[]{:S(2)}, u32[]{:S(2)}) async-start(bf16[16,2,1,12,2048]{4,1,3,2,0:T(2,128)(2,1)} %copy.142), calls=%async_computation.5 | async-start | bytes 3145728 | tf_op jit(solution)/shard_map/all_to_all | solution.py:43
  281.8 67.1 %all-to-all-done.5 = bf16[16,2,1,12,2048]{4,1,3,2,0:T(2,128)(2,1)S(1)} async-done(((bf16[16,2,1,12,2048]{4,1,3,2,0:T(2,128)(2,1)}), bf16[16,2,1,12,2048]{4,1,3,2,0:T(2,128)(2,1)S(1)}, u32[]{:S(2)}, u32[]{:S(2)}) %all-to-all-start.5) | async-done | bytes 1572896 | tf_op jit(solution)/shard_map/all_to_all | solution.py:43
  351.0 2.5 reshape_reshape_reshape.7
  353.5 2.3 gather_fusion.8
  355.8 2.4 gather_fusion.7
  358.2 2.4 gather_fusion.6
  360.6 2.3 gather_fusion.5
  362.9 2.3 gather_fusion.4
  365.2 2.3 gather_fusion.3
  367.6 2.4 gather_fusion.2
  370.0 2.3 gather_fusion.1
  372.3 4.4 %fusion.26 = bf16[16,256,128]{2,1,0:T(8,128)(2,1)S(1)} fusion(f32[256]{0:T(256)S(1)} %get-tuple-element.147, f32[256]{0:T(256)S(1)} %get-tuple-element.148, f32[256]{0:T(256)S(1)} %get-tuple-element.149, f32[256]{0:T(256)S(1)} %get-tuple-element.150, f32[256]{0:T(256)S(1)} %get-tuple-element.151, f32[256]{0:T(256)S(1)} %get-tuple-element.152, ...), kind=kLoop, calls=%fused_computation.75 | loop fusion | flops 12582912 | bytes 9445376 | tf_op jit(solution)/shard_map/transpose | solution.py:36
  376.7 15.9 %all_to_all.38 = bf16[16,256,128]{2,1,0:T(8,128)(2,1)S(1)} all-to-all(bf16[16,256,128]{2,1,0:T(8,128)(2,1)S(1)} %fusion.26), channel_id=1, replica_groups=mesh['sp_0'=16,'sp_1'=2,'tp'=16] {'tp'}, dimensions={0} | all-to-all | bytes 2097152 | tf_op jit(solution)/shard_map/all_to_all | solution.py:61
  (132 shorter events, 57.6 us)
Async XLA Ops:
  6.5 241.1 %copy-start = (bf16[1,256,2048]{2,1,0:T(8,128)(2,1)S(1)}, bf16[1,256,2048]{2,1,0:T(8,128)(2,1)}, u32[]{:S(2)}) copy-start(bf16[1,256,2048]{2,1,0:T(8,128)(2,1)} %param.25) | copy-start | bytes 3145732
  6.5 80.9 %all-gather.2.cloned.1.call-start = ((), (), s32[]{:S(2)}) async-start(), calls=%async_computation.7 | async-start | bytes 2162688 | tf_op jit(solution)/shard_map/all_gather | solution.py:153
  114.3 23.6 %all-to-all-start = ((bf16[16,256,128]{1,2,0:T(8,128)(2,1)}), bf16[16,256,128]{1,2,0:T(8,128)(2,1)}, u32[]{:S(2)}, u32[]{:S(2)}) async-start(bf16[16,256,128]{1,2,0:T(8,128)(2,1)} %broadcast_in_dim.47), calls=%async_computation | async-start | bytes 2097152 | tf_op jit(solution)/shard_map/all_to_all | solution.py:26
  122.2 15.7 %copy-start.2 = (bf16[256,128]{1,0:T(8,128)(2,1)S(1)}, bf16[256,128]{1,0:T(8,128)(2,1)}, u32[]{:S(2)}) copy-start(bf16[256,128]{1,0:T(8,128)(2,1)} %param.19) | copy-start | bytes 196612
  140.9 21.0 %all-to-all-start.1 = ((bf16[16,256,128]{2,1,0:T(8,128)(2,1)}), bf16[16,256,128]{2,1,0:T(8,128)(2,1)}, u32[]{:S(2)}, u32[]{:S(2)}) async-start(bf16[16,256,128]{2,1,0:T(8,128)(2,1)} %broadcast_in_dim.49), calls=%async_computation.1 | async-start | bytes 2097152 | tf_op jit(solution)/shard_map/all_to_all | solution.py:26
  224.0 15.4 %collective-permute-start = (bf16[32,6,2048]{2,0,1:T(8,128)(2,1)S(1)}, bf16[32,6,2048]{2,0,1:T(8,128)(2,1)S(1)}, u32[]{:S(2)}, u32[]{:S(2)}) collective-permute-start(bf16[32,6,2048]{2,0,1:T(8,128)(2,1)S(1)} %reshape_reshape.7), channel_id=1, source_target_pairs={{0,1},{1,0},{2,3},{3,2},{4,5},{5,4},{6,7},{7,6},{8,9},{9,8},{10,11... | collective-permute-start | bytes 2359304 | tf_op jit(solution)/shard_map/ppermute | solution.py:56
  245.2 2.4 copy-start.1
  262.9 12.2 %copy-start.3 = (f32[256,8]{0,1:T(8,128)S(1)}, f32[256,8]{0,1:T(8,128)}, u32[]{:S(2)}) copy-start(f32[256,8]{0,1:T(8,128)} %param.22) | copy-start | bytes 24580
  262.9 86.0 %all-to-all-start.5 = ((bf16[16,2,1,12,2048]{4,1,3,2,0:T(2,128)(2,1)}), bf16[16,2,1,12,2048]{4,1,3,2,0:T(2,128)(2,1)S(1)}, u32[]{:S(2)}, u32[]{:S(2)}) async-start(bf16[16,2,1,12,2048]{4,1,3,2,0:T(2,128)(2,1)} %copy.142), calls=%async_computation.5 | async-start | bytes 3145728 | tf_op jit(solution)/shard_map/all_to_all | solution.py:43
Sparse Core Ops, SparseCore 0:
  10.1 77.2 all-gather.1
where the time goes:
time: 402 us; the launch traced here: 400 us
  waiting for transfers between devices  173 us (43%)
  blocking collectives  73.5 us (18%)
  local copies, waits for them, and re-layouts  61.2 us (15%)
  matrix products  30.6 us (8%)
  starting transfers between devices  28.4 us (7%)
  other arithmetic  19.1 us (5%)
  between operations  13.9 us (3%)
    all_gather x1, waiting for transfers between devices, local(): incoming = lax.all_gather(packed, SP, axis=0, tiled=True)  74.1 us
    all_to_all x1, waiting for transfers between devices, turned_blocks(): lax.all_to_all(pieces, axes[k], split_axis=k, concat_axis=k, tiled=True)  67.1 us
    all_to_all x3, blocking collectives, turned_blocks(): lax.all_to_all(pieces, axes[k], split_axis=k, concat_axis=k, tiled=True)  57.5 us
    all_to_all x2, waiting for transfers between devices, from_everyone(): lax.all_to_all(jnp.broadcast_to(x[None], (devices, *x.shape)), axis, 0, 0...  20.5 us
    gather x8, local copies, waits for them, and re-layouts, local(): picked = slot_results[index].astype(jnp.float32)  18.8 us
    all_to_all x1, blocking collectives, summed_on_arrival(): pieces = lax.all_to_all(cut_along(x, dim, devices), axis, 0, 0, tiled=True)  15.9 us
    all_to_all x2, starting transfers between devices, from_everyone(): lax.all_to_all(jnp.broadcast_to(x[None], (devices, *x.shape)), axis, 0, 0...  13.1 us
    ppermute x1, waiting for transfers between devices, swapped(): return lax.ppermute(value, axis, pairs)  11.6 us
  transfers between devices with their start and end apart: 5, of which 5 were waited for; matrix products, arithmetic and copies ran while one was open for 5% of the time, Pallas kernels for 0%

commit v1 on v0

--- a/solution.py
+++ b/solution.py
@@ -150,7 +150,9 @@
         jnp.zeros((local_kv, group_size, token_count), jnp.float32),
         jnp.zeros((local_kv, group_size, token_count, HEAD_DIM), jnp.float32),
     )
-    incoming = lax.all_gather(packed, SP, axis=0, tiled=True)
+    incoming = jnp.concatenate(
+        jax.lax.all_to_all(jnp.stack(jax.lax.axis_size(SP) * [packed], axis=0), SP, 0, 0), axis=0
+    )
     incoming_len = incoming.shape[0]
     step_len = math.gcd(incoming_len, KEY_BLOCK)
 

time: 402 us -> 415 us (1.032)
  waiting for transfers between devices: 173 us -> 200 us
  starting transfers between devices: 28.4 us -> 44.8 us
  matrix products: 30.6 us -> 16.7 us
  between operations: 13.9 us -> 0.59 us
    all_to_all x0 -> x1, waiting for transfers between devices: none -> 97.2 us  [local(): jax.lax.all_to_all(jnp.stack(jax.lax.axis_size(SP) * [packed], axis=0), S...]
    all_gather x1 -> x0, waiting for transfers between devices: 74.1 us -> none  [local(): incoming = lax.all_gather(packed, SP, axis=0, tiled=True)]
    all_to_all x0 -> x1, starting transfers between devices: none -> 15.7 us  [local(): jax.lax.all_to_all(jnp.stack(jax.lax.axis_size(SP) * [packed], axis=0), S...]
    dot_general x8, matrix products: 11 us -> 3.37 us  [online_update(): jnp.einsum('tkgd,nkd->kgtn', query_groups, key_block, preferred_element_t...]
    dot_general x8, matrix products: 11.1 us -> 4.86 us  [online_update(): jnp.einsum('kgtn,nkd->kgtd', weights, value_block, preferred_element_type...]
    all_to_all x1, waiting for transfers between devices: 67.1 us -> 71.6 us  [turned_blocks(): lax.all_to_all(pieces, axes[k], split_axis=k, concat_axis=k, tiled=True)]
  transfers between devices with their start and end apart: 5 -> 5, of which waited for: 5 -> 5; matrix products, arithmetic and copies ran while one was open for 5% -> 4% of each run, Pallas kernels for 0% -> 0%
where the time goes in v1:
time: 415 us; the launch traced here: 414 us
  waiting for transfers between devices  200 us (48%)
  blocking collectives  73.6 us (18%)
  local copies, waits for them, and re-layouts  61.8 us (15%)
  starting transfers between devices  44.8 us (11%)
  matrix products  16.7 us (4%)
  other arithmetic  16.6 us (4%)
    all_to_all x1, waiting for transfers between devices, local(): jax.lax.all_to_all(jnp.stack(jax.lax.axis_size(SP) * [packed], axis=0), S...  97.2 us
    all_to_all x1, waiting for transfers between devices, turned_blocks(): lax.all_to_all(pieces, axes[k], split_axis=k, concat_axis=k, tiled=True)  71.6 us
    all_to_all x3, blocking collectives, turned_blocks(): lax.all_to_all(pieces, axes[k], split_axis=k, concat_axis=k, tiled=True)  57.4 us
    all_to_all x2, waiting for transfers between devices, from_everyone(): lax.all_to_all(jnp.broadcast_to(x[None], (devices, *x.shape)), axis, 0, 0...  19.2 us
    gather x8, local copies, waits for them, and re-layouts, local(): picked = slot_results[index].astype(jnp.float32)  18.8 us
    all_to_all x1, blocking collectives, summed_on_arrival(): pieces = lax.all_to_all(cut_along(x, dim, devices), axis, 0, 0, tiled=True)  16.2 us
    all_to_all x1, starting transfers between devices, local(): jax.lax.all_to_all(jnp.stack(jax.lax.axis_size(SP) * [packed], axis=0), S...  15.7 us
    all_to_all x2, starting transfers between devices, from_everyone(): lax.all_to_all(jnp.broadcast_to(x[None], (devices, *x.shape)), axis, 0, 0...  13.7 us
  transfers between devices with their start and end apart: 5, of which 5 were waited for; matrix products, arithmetic and copies ran while one was open for 4% of the time, Pallas kernels for 0%

profile of v1, /device:TPU:2, one launch (start us, length us, event | category | flops | bytes accessed | tf_op | source)
XLA Modules:
  0.0 414.1 jit_solution(1621782154902845675)
XLA Ops:
  4.3 15.7 %all-to-all-start = ((bf16[32,256,128]{1,2,0:T(8,128)(2,1)}), bf16[32,256,128]{1,2,0:T(8,128)(2,1)}, u32[]{:S(2)}, u32[]{:S(2)}) async-start(bf16[32,256,128]{1,2,0:T(8,128)(2,1)} %stack.20), calls=%async_computation | async-start | bytes 4194304 | tf_op jit(solution)/shard_map/all_to_all | solution.py:154
  21.8 97.2 %all-to-all-done = bf16[32,256,128]{1,2,0:T(8,128)(2,1)} async-done(((bf16[32,256,128]{1,2,0:T(8,128)(2,1)}), bf16[32,256,128]{1,2,0:T(8,128)(2,1)}, u32[]{:S(2)}, u32[]{:S(2)}) %all-to-all-start) | async-done | bytes 2097184 | tf_op jit(solution)/shard_map/all_to_all | solution.py:154
  119.0 3.2 copy.126
  122.2 11.8 %while.18 = (s32[]{:T(128)}, f32[1,2,256]{2,1,0:T(2,128)S(1)}, f32[1,2,256]{2,1,0:T(2,128)S(1)}, f32[1,2,256,64]{2,3,1,0:T(8,128)S(1)}, bf16[8192,128]{1,0:T(8,1...) while((s32[]{:T(128)}, f32[1,2,256]{2,1,0:T(2,128)S(1)}, ...), condition=%wide.region_5.6_spmd.clone, body=%wide.region_2.5_spmd.clone.sunk | while | flops 139561984 | bytes 7176391 | solution.py:165
  135.2 7.5 %all-to-all-start.1 = ((bf16[16,256,128]{1,2,0:T(8,128)(2,1)}), bf16[16,256,128]{1,2,0:T(8,128)(2,1)}, u32[]{:S(2)}, u32[]{:S(2)}) async-start(bf16[16,256,128]{1,2,0:T(8,128)(2,1)} %broadcast_in_dim.47), calls=%async_computation.1 | async-start | bytes 2097152 | tf_op jit(solution)/shard_map/all_to_all | solution.py:26
  144.5 13.8 %all-to-all-done.1 = bf16[16,256,128]{1,2,0:T(8,128)(2,1)} async-done(((bf16[16,256,128]{1,2,0:T(8,128)(2,1)}), bf16[16,256,128]{1,2,0:T(8,128)(2,1)}, u32[]{:S(2)}, u32[]{:S(2)}) %all-to-all-start.1) | async-done | bytes 1048608 | tf_op jit(solution)/shard_map/all_to_all | solution.py:26
  161.4 6.2 %all-to-all-start.2 = ((bf16[16,256,128]{2,1,0:T(8,128)(2,1)}), bf16[16,256,128]{2,1,0:T(8,128)(2,1)}, u32[]{:S(2)}, u32[]{:S(2)}) async-start(bf16[16,256,128]{2,1,0:T(8,128)(2,1)} %broadcast_in_dim.49), calls=%async_computation.2 | async-start | bytes 2097152 | tf_op jit(solution)/shard_map/all_to_all | solution.py:26
  168.6 8.0 %scatter_custom_fusion = s32[385]{0:T(512)S(1)} fusion(s32[2048]{0:T(1024)S(1)} %bitcast.226, s32[2048]{0:T(1024)S(1)} %add_select_fusion.2, s32[]{:T(128)} %constant.176.clone.1), kind=kCustom, calls=%fused_computation.181 | custom fusion | bytes 1544 | tf_op jit(solution)/shard_map/scatter | solution.py:194
  176.7 5.4 %all-to-all-done.2 = bf16[16,256,128]{2,1,0:T(8,128)(2,1)} async-done(((bf16[16,256,128]{2,1,0:T(8,128)(2,1)}), bf16[16,256,128]{2,1,0:T(8,128)(2,1)}, u32[]{:S(2)}, u32[]{:S(2)}) %all-to-all-start.2) | async-done | bytes 1048608 | tf_op jit(solution)/shard_map/all_to_all | solution.py:26
  183.6 3.1 gather_fusion
  186.7 2.4 reshape.668
  189.9 4.4 %all_to_all.40 = bf16[16,2,1,6,2048]{4,0,3,2,1:T(8,128)(2,1)S(1)} all-to-all(bf16[16,2,1,6,2048]{4,0,3,2,1:T(8,128)(2,1)S(1)} %copy.140), channel_id=1, replica_groups=mesh['sp_0'=16,'sp_1'=2,'tp'=16] {'sp_1'}, dimensions={1} | all-to-all | bytes 1572864 | tf_op jit(solution)/shard_map/all_to_all | solution.py:43
  195.1 48.0 %all_to_all.41 = bf16[16,2,1,6,2048]{4,1,3,2,0:T(2,128)(2,1)S(1)} all-to-all(bf16[16,2,1,6,2048]{4,1,3,2,0:T(2,128)(2,1)S(1)} %copy.141), channel_id=1, replica_groups=mesh['sp_0'=16,'sp_1'=2,'tp'=16] {'sp_0'}, dimensions={0} | all-to-all | bytes 1572864 | tf_op jit(solution)/shard_map/all_to_all | solution.py:43
  244.0 3.9 collective-permute-start
  248.0 11.8 %collective-permute-done = bf16[32,6,2048]{2,0,1:T(8,128)(2,1)S(1)} collective-permute-done((bf16[32,6,2048]{2,0,1:T(8,128)(2,1)S(1)}, bf16[32,6,2048]{2,0,1:T(8,128)(2,1)S(1)}, u32[]{:S(2)}, u32[]{:S(2)}) %collective-permute-start) | collective-permute-done | bytes 786464 | tf_op jit(solution)/shard_map/ppermute | solution.py:56
  265.5 2.4 convolution_multiply_fusion
  267.9 4.2 %convolution_convert_fusion = bf16[384,2048]{1,0:T(8,128)(2,1)} fusion(bf16[1,256,2048]{2,1,0:T(8,128)(2,1)S(1)} %copy-done, f32[384,256]{1,0:T(8,128)S(1)} %convolution_multiply_fusion, bf16[384,2048]{1,0:T(8,128)(2,1)S(1)} %copy-done.2, bf16[1,2048,256]{2,1,0:T(8,128)(2,1)} %param.23, f32[384]{0:T(512)S(1)} %rsqrt.30), kind=kOutput, calls=%fused_computation.32 | convolution fusion | flops 806780928 | bytes 5637632 | tf_op jit(solution)/shard_map/dot_general | solution.py:215
  272.1 2.4 reshape_reshape_reshape.6
  275.4 5.0 %all_to_all.42 = bf16[16,2,1,12,2048]{4,0,3,2,1:T(8,128)(2,1)S(1)} all-to-all(bf16[16,2,1,12,2048]{4,0,3,2,1:T(8,128)(2,1)S(1)} %copy.145), channel_id=1, replica_groups=mesh['sp_0'=16,'sp_1'=2,'tp'=16] {'sp_1'}, dimensions={1} | all-to-all | bytes 3145728 | tf_op jit(solution)/shard_map/all_to_all | solution.py:43
  280.4 2.8 copy.146
  283.2 11.4 %all-to-all-start.6 = ((bf16[16,2,1,12,2048]{4,1,3,2,0:T(2,128)(2,1)}), bf16[16,2,1,12,2048]{4,1,3,2,0:T(2,128)(2,1)S(1)}, u32[]{:S(2)}, u32[]{:S(2)}) async-start(bf16[16,2,1,12,2048]{4,1,3,2,0:T(2,128)(2,1)} %copy.146), calls=%async_computation.6 | async-start | bytes 3145728 | tf_op jit(solution)/shard_map/all_to_all | solution.py:43
  297.6 71.6 %all-to-all-done.6 = bf16[16,2,1,12,2048]{4,1,3,2,0:T(2,128)(2,1)S(1)} async-done(((bf16[16,2,1,12,2048]{4,1,3,2,0:T(2,128)(2,1)}), bf16[16,2,1,12,2048]{4,1,3,2,0:T(2,128)(2,1)S(1)}, u32[]{:S(2)}, u32[]{:S(2)}) %all-to-all-start.6) | async-done | bytes 1572896 | tf_op jit(solution)/shard_map/all_to_all | solution.py:43
  371.3 2.5 reshape_reshape_reshape.7
  373.8 2.3 gather_fusion.8
  376.1 2.4 gather_fusion.7
  378.5 2.4 gather_fusion.6
  383.2 2.3 gather_fusion.4
  385.5 2.3 gather_fusion.3
  387.9 2.4 gather_fusion.2
  390.3 2.3 gather_fusion.1
  392.6 4.4 %fusion.26 = bf16[16,256,128]{2,1,0:T(8,128)(2,1)S(1)} fusion(f32[256]{0:T(256)S(1)} %get-tuple-element.159, f32[256]{0:T(256)S(1)} %get-tuple-element.160, f32[256]{0:T(256)S(1)} %get-tuple-element.161, f32[256]{0:T(256)S(1)} %get-tuple-element.162, f32[256]{0:T(256)S(1)} %get-tuple-element.163, f32[256]{0:T(256)S(1)} %get-tuple-element.164, ...), kind=kLoop, calls=%fused_computation.75 | loop fusion | flops 12582912 | bytes 9445376 | tf_op jit(solution)/shard_map/transpose | solution.py:36
  397.1 16.2 %all_to_all.43 = bf16[16,256,128]{2,1,0:T(8,128)(2,1)S(1)} all-to-all(bf16[16,256,128]{2,1,0:T(8,128)(2,1)S(1)} %fusion.26), channel_id=1, replica_groups=mesh['sp_0'=16,'sp_1'=2,'tp'=16] {'tp'}, dimensions={0} | all-to-all | bytes 2097152 | tf_op jit(solution)/shard_map/all_to_all | solution.py:61
  (143 shorter events, 43.1 us)
Async XLA Ops:
  0.0 267.9 %copy-start = (bf16[1,256,2048]{2,1,0:T(8,128)(2,1)S(1)}, bf16[1,256,2048]{2,1,0:T(8,128)(2,1)}, u32[]{:S(2)}) copy-start(bf16[1,256,2048]{2,1,0:T(8,128)(2,1)} %param.25) | copy-start | bytes 3145732
  4.3 15.8 %copy-start.6 = (s32[256,8]{0,1:T(8,128)S(1)}, s32[256,8]{0,1:T(8,128)}, u32[]{:S(2)}) copy-start(s32[256,8]{0,1:T(8,128)} %param.21) | copy-start | bytes 24580
  4.3 16.9 %copy-start.8 = (f32[2,64]{1,0:T(2,128)S(1)}, f32[2,64]{1,0:T(2,128)}, u32[]{:S(2)}) copy-start(f32[2,64]{1,0:T(2,128)} %param.17) | copy-start | bytes 1540
  4.3 17.0 %copy-start.4 = (bf16[256,128]{1,0:T(8,128)(2,1)S(1)}, bf16[256,128]{1,0:T(8,128)(2,1)}, u32[]{:S(2)}) copy-start(bf16[256,128]{1,0:T(8,128)(2,1)} %param.14) | copy-start | bytes 196612
  4.3 114.7 %all-to-all-start = ((bf16[32,256,128]{1,2,0:T(8,128)(2,1)}), bf16[32,256,128]{1,2,0:T(8,128)(2,1)}, u32[]{:S(2)}, u32[]{:S(2)}) async-start(bf16[32,256,128]{1,2,0:T(8,128)(2,1)} %stack.20), calls=%async_computation | async-start | bytes 4194304 | tf_op jit(solution)/shard_map/all_to_all | solution.py:154
  135.2 23.1 %all-to-all-start.1 = ((bf16[16,256,128]{1,2,0:T(8,128)(2,1)}), bf16[16,256,128]{1,2,0:T(8,128)(2,1)}, u32[]{:S(2)}, u32[]{:S(2)}) async-start(bf16[16,256,128]{1,2,0:T(8,128)(2,1)} %broadcast_in_dim.47), calls=%async_computation.1 | async-start | bytes 2097152 | tf_op jit(solution)/shard_map/all_to_all | solution.py:26
  143.3 15.0 %copy-start.3 = (bf16[256,128]{1,0:T(8,128)(2,1)S(1)}, bf16[256,128]{1,0:T(8,128)(2,1)}, u32[]{:S(2)}) copy-start(bf16[256,128]{1,0:T(8,128)(2,1)} %param.19) | copy-start | bytes 196612
  161.4 7.1 %copy-start.5 = (s32[2048,1]{0,1:T(1,128)S(1)}, s32[2048,1]{0,1:T(1,128)}, u32[]{:S(2)}) copy-start(s32[2048,1]{0,1:T(1,128)} %reshape.666) | copy-start | bytes 24580
  161.4 20.7 %all-to-all-start.2 = ((bf16[16,256,128]{2,1,0:T(8,128)(2,1)}), bf16[16,256,128]{2,1,0:T(8,128)(2,1)}, u32[]{:S(2)}, u32[]{:S(2)}) async-start(bf16[16,256,128]{2,1,0:T(8,128)(2,1)} %broadcast_in_dim.49), calls=%async_computation.2 | async-start | bytes 2097152 | tf_op jit(solution)/shard_map/all_to_all | solution.py:26
  244.0 15.7 %collective-permute-start = (bf16[32,6,2048]{2,0,1:T(8,128)(2,1)S(1)}, bf16[32,6,2048]{2,0,1:T(8,128)(2,1)S(1)}, u32[]{:S(2)}, u32[]{:S(2)}) collective-permute-start(bf16[32,6,2048]{2,0,1:T(8,128)(2,1)S(1)} %reshape_reshape.7), channel_id=1, source_target_pairs={{0,1},{1,0},{2,3},{3,2},{4,5},{5,4},{6,7},{7,6},{8,9},{9,8},{10,11... | collective-permute-start | bytes 2359304 | tf_op jit(solution)/shard_map/ppermute | solution.py:56
  265.5 2.4 copy-start.2
  283.2 11.6 %copy-start.7 = (f32[256,8]{0,1:T(8,128)S(1)}, f32[256,8]{0,1:T(8,128)}, u32[]{:S(2)}) copy-start(f32[256,8]{0,1:T(8,128)} %param.22) | copy-start | bytes 24580
  283.2 86.0 %all-to-all-start.6 = ((bf16[16,2,1,12,2048]{4,1,3,2,0:T(2,128)(2,1)}), bf16[16,2,1,12,2048]{4,1,3,2,0:T(2,128)(2,1)S(1)}, u32[]{:S(2)}, u32[]{:S(2)}) async-start(bf16[16,2,1,12,2048]{4,1,3,2,0:T(2,128)(2,1)} %copy.146), calls=%async_computation.6 | async-start | bytes 3145728 | tf_op jit(solution)/shard_map/all_to_all | solution.py:43
  392.6 21.5 %copy-start.1 = (bf16[1,256,2048]{2,1,0:T(8,128)(2,1)S(1)}, bf16[1,256,2048]{2,1,0:T(8,128)(2,1)}, u32[]{:S(2)}) copy-start(bf16[1,256,2048]{2,1,0:T(8,128)(2,1)} %param.25) | copy-start | bytes 3145732
